TPU v7x, 128 devices: a whole 4x4x4 slice. The times are simulated.
128 devices in a mesh: sp: 32 (over z, y, core), tp: 4 (over x).
Axes of the slice: x: 4, y: 4, z: 4, core: 2. Of those that a mesh axis runs over, the one named last changes fastest.
Arguments:
- residual: bfloat16 [32768, 2048], P('sp'), may hold values from -8 to 8
- query_wide: bfloat16 [32768, 1024], P('sp', 'tp'), may hold values from -6 to 6
- key_wide: bfloat16 [32768, 1024], P('sp', 'tp'), may hold values from -6 to 6
- value_wide: bfloat16 [32768, 2048], P('sp', 'tp'), may hold values from -6 to 6
- decay_wide: bfloat16 [32768, 1024], P('sp', 'tp'), may hold values from -12 to 12
- gate_wide: bfloat16 [32768, 2048], P('sp', 'tp'), may hold values from -6 to 6
- query_narrow: bfloat16 [32768, 512], P('sp', 'tp'), may hold values from -6 to 6
- key_narrow: bfloat16 [32768, 512], P('sp', 'tp'), may hold values from -6 to 6
- value_narrow: bfloat16 [32768, 2048], P('sp', 'tp'), may hold values from -6 to 6
- decay_narrow: bfloat16 [32768, 512], P('sp', 'tp'), may hold values from -12 to 12
- gate_narrow: bfloat16 [32768, 2048], P('sp', 'tp'), may hold values from -6 to 6
- head_gain: float32 [512], replicated, may hold values from 0.1 to 1.9
- out_wide: bfloat16 [2048, 2048], P('tp'), may hold values from -0.125 to 0.125
- out_narrow: bfloat16 [2048, 2048], P('tp'), may hold values from -0.125 to 0.125
- mlp_gain: float32 [2048], replicated, may hold values from 0.1 to 1.9
- up_weight: bfloat16 [2048, 4096], P('sp', 'tp'), may hold values from -0.125 to 0.125
- down_weight: bfloat16 [4096, 2048], P('tp', 'sp'), may hold values from -0.09375 to 0.09375
Outputs:
- layer_out: bfloat16 [32768, 2048], P('sp', 'tp')
All inputs are finite; a program needn't handle non-finite values.
Results may differ from a plain program's by a relative error of at most 0.017.
Values may be sent and summed in bfloat16 or wider, within the bound.
A program may use at most 128 MiB of HBM per device.

v0:
```python
import jax
import jax.numpy as jnp
from jax import lax
from jax.sharding import PartitionSpec as P

HEADS = 4
BLOCK = 64
EPS = 1e-05
DECAY_NORMALIZER = 16.0
HIGHEST = lax.Precision.HIGHEST


def turned_gather(arrays, axis, dims):
    turned = [jnp.moveaxis(a, dim, 0) for a, dim in zip(arrays, dims)]
    both = jnp.concatenate([t.reshape(len(t), -1) for t in turned], axis=1)
    whole, at, finished = (lax.all_gather(both, axis, axis=0, tiled=True), 0, [])
    for t, dim in zip(turned, dims):
        section = whole[:, at : at + t[0].size].reshape(-1, *t.shape[1:])
        finished.append(jnp.moveaxis(section, 0, dim))
        at += t[0].size
    return tuple(finished)


def entering(array, axis, join, neutral):
    place = lax.axis_index(axis)
    gathered = jax.tree.map(
        lambda a, kind: lax.all_gather(a.astype(kind), axis),
        array,
        (jnp.bfloat16, jnp.bfloat16, jnp.bfloat16, jnp.bfloat16),
    )
    state = jax.tree.map(lambda a, e: jnp.zeros_like(a) + jnp.asarray(e, a.dtype), array, neutral)

    def one(step, state):
        return join(
            state,
            jax.tree.map(
                lambda a, own: lax.dynamic_index_in_dim(a, step, 0, False).astype(own.dtype),
                gathered,
                array,
            ),
        )

    return lax.fori_loop(0, place, one, state)


def split_up(array, dim, count):
    dims = array.shape
    pieces = array.reshape(*dims[:dim], count, dims[dim] // count, *dims[dim + 1 :])
    return jnp.moveaxis(pieces, dim, 0)


def sum_at_owner(array, axis, dim):
    count = lax.axis_size(axis)
    pieces = lax.all_to_all(split_up(array, dim, count), axis, 0, 0, tiled=True)
    return jnp.sum(pieces.astype(jnp.float32), axis=0)


def sent_to_all(array, axis):
    copies = jnp.broadcast_to(array, (lax.axis_size(axis), *array.shape))
    return lax.all_to_all(copies, axis, split_axis=0, concat_axis=0, tiled=True)


def of_everyone(array, axis):
    everything = sent_to_all(array, axis)
    return jnp.sum(everything, axis=0)


def block_pass(queries, keys_in, values_in, log_decay, block_len):
    num_blocks = queries.shape[0] // block_len

    def to_blocks(stacked):
        return stacked.reshape((num_blocks, block_len) + stacked.shape[1:])

    causal = jnp.tril(jnp.ones((block_len, block_len), dtype=bool))
    initial = (
        jnp.zeros((queries.shape[1], queries.shape[2], values_in.shape[2]), jnp.float32),
        jnp.zeros((queries.shape[1], queries.shape[2]), jnp.float32),
    )

    def advance(running, inputs):
        memory, offset = running
        block_q, block_k, block_v, block_g = inputs
        within = jnp.cumsum(block_g, axis=0)
        final_log = within[-1]
        scaled_q = block_q * jnp.exp(within)
        scaled_k = block_k * jnp.exp(-within)
        outside = jnp.einsum("ihd,hde->ihe", scaled_q, memory, precision=HIGHEST)
        scores = jnp.einsum("ihd,jhd->hij", scaled_q, scaled_k, precision=HIGHEST)
        scores = jnp.where(causal[None], scores, 0.0)
        inside = jnp.einsum("hij,jhe->ihe", scores, block_v, precision=HIGHEST)
        decayed_keys = scaled_k * jnp.exp(final_log)[None]
        memory = jnp.exp(final_log)[..., None] * memory + jnp.einsum(
            "jhd,jhe->hde", decayed_keys, block_v, precision=HIGHEST
        )
        carried_q = scaled_q * jnp.exp(offset)[None]
        return ((memory, offset + final_log), (outside + inside, carried_q))

    (memory, totals), (outputs, carried_q) = lax.scan(
        advance,
        initial,
        (to_blocks(queries), to_blocks(keys_in), to_blocks(values_in), to_blocks(log_decay)),
    )
    return (outputs.reshape(values_in.shape), carried_q.reshape(queries.shape), totals, memory)


def prepare(query, key_proj, value, decay, heads_here):
    row_count = query.shape[0]
    key_width = query.shape[1] // heads_here
    queries = query.astype(jnp.float32).reshape(row_count, heads_here, key_width) * key_width ** (
        -0.5
    )
    keys_in = key_proj.astype(jnp.float32).reshape(row_count, heads_here, key_width)
    values_in = value.astype(jnp.float32).reshape(
        row_count, heads_here, value.shape[1] // heads_here
    )
    log_decay = (
        jax.nn.log_sigmoid(decay.astype(jnp.float32)).reshape(row_count, heads_here, key_width)
        / DECAY_NORMALIZER
    )
    return (queries, keys_in, values_in, log_decay)


def finish(outputs, gate, head_gain):
    scale = lax.rsqrt(jnp.mean(jnp.square(outputs), axis=-1, keepdims=True) + EPS)
    gated = (
        outputs * scale * head_gain * jax.nn.silu(gate.astype(jnp.float32).reshape(outputs.shape))
    )
    return gated.reshape(outputs.shape[0], -1).astype(jnp.bfloat16)


def combine_states(earlier, later):
    return (
        earlier[0] + later[0],
        jnp.exp(later[0])[..., None] * earlier[1] + later[1],
        earlier[2] + later[2],
        jnp.exp(later[2])[..., None] * earlier[3] + later[3],
    )


def body(
    residual,
    query_wide,
    key_wide,
    value_wide,
    decay_wide,
    gate_wide,
    query_narrow,
    key_narrow,
    value_narrow,
    decay_narrow,
    gate_narrow,
    head_gain,
    out_wide,
    out_narrow,
    mlp_gain,
    up_weight,
    down_weight,
):
    heads_here = HEADS // lax.axis_size("tp")
    up_whole, down_whole = turned_gather((up_weight, down_weight), "sp", (0, 1))
    wq, wk, wv, wg = prepare(query_wide, key_wide, value_wide, decay_wide, heads_here)
    wide_out, wide_q, wide_total, wide_memory = block_pass(wq, wk, wv, wg, BLOCK)
    nq, nk, nv, ng = prepare(query_narrow, key_narrow, value_narrow, decay_narrow, heads_here)
    narrow_out, narrow_q, narrow_total, narrow_memory = block_pass(nq, nk, nv, ng, BLOCK)
    identity = (
        jnp.zeros_like(wide_total),
        jnp.zeros_like(wide_memory),
        jnp.zeros_like(narrow_total),
        jnp.zeros_like(narrow_memory),
    )
    incoming = entering(
        (wide_total, wide_memory, narrow_total, narrow_memory), "sp", combine_states, identity
    )
    wide_out = wide_out + jnp.einsum("ihd,hde->ihe", wide_q, incoming[1], precision=HIGHEST)
    narrow_out = narrow_out + jnp.einsum("ihd,hde->ihe", narrow_q, incoming[3], precision=HIGHEST)
    gated_wide = finish(wide_out, gate_wide, head_gain)
    gated_narrow = finish(narrow_out, gate_narrow, head_gain)
    head_terms = jnp.dot(gated_wide, out_wide, preferred_element_type=jnp.float32) + jnp.dot(
        gated_narrow, out_narrow, preferred_element_type=jnp.float32
    )
    tp_index = lax.axis_index("tp")
    col_count = residual.shape[1] // lax.axis_size("tp")
    full_width = residual.shape[1]
    residual_cols = lax.dynamic_slice_in_dim(residual, tp_index * col_count, col_count, 1)
    mixed_cols = sum_at_owner(head_terms.astype(jnp.bfloat16), "tp", 1)
    stream_cols = (residual_cols.astype(jnp.float32) + mixed_cols).astype(jnp.bfloat16)
    stream_f = stream_cols.astype(jnp.float32)
    squares = of_everyone(jnp.sum(jnp.square(stream_f), axis=1, keepdims=True), "tp")
    gain_cols = lax.dynamic_slice_in_dim(mlp_gain, tp_index * col_count, col_count, 0)
    normed_cols = (stream_f * lax.rsqrt(squares / full_width + EPS) * gain_cols).astype(
        jnp.bfloat16
    )
    normed = lax.all_gather(normed_cols, "tp", axis=1, tiled=True)
    before_activation = jnp.dot(normed, up_whole, preferred_element_type=jnp.float32)
    hidden = jnp.square(jax.nn.relu(before_activation)).astype(jnp.bfloat16)
    down_terms = jnp.dot(hidden, down_whole, preferred_element_type=jnp.float32)
    mlp_cols = sum_at_owner(down_terms.astype(jnp.bfloat16), "tp", 1)
    return (stream_cols.astype(jnp.float32) + mlp_cols).astype(jnp.bfloat16)


def solution(mesh):
    return jax.shard_map(
        body,
        mesh=mesh,
        in_specs=(
            P("sp", None),
            P("sp", "tp"),
            P("sp", "tp"),
            P("sp", "tp"),
            P("sp", "tp"),
            P("sp", "tp"),
            P("sp", "tp"),
            P("sp", "tp"),
            P("sp", "tp"),
            P("sp", "tp"),
            P("sp", "tp"),
            P(),
            P("tp", None),
            P("tp", None),
            P(),
            P("sp", "tp"),
            P("tp", "sp"),
        ),
        out_specs=P("sp", "tp"),
        check_vma=False,
    )
```

profile of v0, /device:TPU:0, one launch (start us, length us, event | category | flops | bytes accessed | tf_op | source)
XLA Modules:
  0.0 539.1 jit_solution(10759921777863404328)
XLA Ops:
  6.6 5.0 reshape.518
  13.8 1.7 broadcast.136.clone.1
  15.4 68.4 %while.51 = (s32[]{:T(128)}, f32[1,128,512]{2,1,0:T(8,128)S(1)}, f32[1,128]{1,0:T(1,128)S(1)}, f32[16,64,1,512]{3,1,2,0:T(8,128)}, f32[16,64,1,128]{3,1,2,0:T(8,...) while((s32[]{:T(128)}, f32[1,128,512]{2,1,0:T(8,128)S(1)}, ...), condition=%wide.region_5.6_spmd.clone, body=%wide.region_3.5_spmd.clone.sunk | while | flops 133005568 | bytes 2333321 | solution.py:98
  84.7 2.7 fusion.90
  87.3 3.3 reshape.501
  91.6 3.4 reshape.502
  95.0 4.9 reshape.516
  99.8 2.0 reshape.515
  101.9 1.6 broadcast.136.clone
  103.5 108.8 %while.50 = (s32[]{:T(128)}, f32[1,256,512]{2,1,0:T(8,128)S(1)}, f32[1,256]{1,0:T(1,128)S(1)}, f32[16,64,1,512]{3,1,2,0:T(8,128)}, f32[16,64,1,256]{3,1,2,0:T(8,...) while((s32[]{:T(128)}, f32[1,256,512]{2,1,0:T(8,128)S(1)}, ...), condition=%wide.region_2.3_spmd.clone, body=%wide.region_0.2_spmd.clone.sunk | while | flops 240787968 | bytes 3648133 | solution.py:98
  213.9 3.0 copy.32
  216.9 1.3 copy.33
  218.2 3.0 copy.34
  221.3 1.4 copy.35
  222.6 23.1 %all-gather.5 = bf16[32,1,128]{2,1,0:T(2,128)(2,1)S(1)} all-gather(bf16[1,1,128]{2,1,0:T(2,128)(2,1)S(1)} %convert_bitcast_fusion.1), channel_id=4, replica_groups=mesh['sp'=32,'tp'=4] {'sp'}, dimensions={0}, use_global_device_ids=true | all-gather | bytes 8448 | tf_op jit(solution)/shard_map/all_gather | solution.py:27
  245.7 23.8 %all-gather.4 = bf16[32,1,256]{2,1,0:T(2,128)(2,1)S(1)} all-gather(bf16[1,1,256]{2,1,0:T(2,128)(2,1)S(1)} %convert_bitcast_fusion), channel_id=2, replica_groups=mesh['sp'=32,'tp'=4] {'sp'}, dimensions={0}, use_global_device_ids=true | all-gather | bytes 16896 | tf_op jit(solution)/shard_map/all_gather | solution.py:27
  269.6 5.6 %multiply_reduce_fusion.1 = (f32[1024]{0:T(1024)S(1)}, f32[1024,1,512]{0,2,1:T(8,128)S(1)}) fusion(f32[1024,1,512]{0,2,1:T(8,128)} %copy.32, f32[1024,256]{1,0:T(8,128)} %bitcast.301, f32[1,256,512]{2,1,0:T(8,128)S(1)} %get-tuple-element.190), kind=kOutput, calls=%fused_computation.128 | convolution fusion | flops 1612184576 | bytes 5771264 | tf_op jit(solution)/shard_map/ihd,hde->ihe/dot_general | solution.py:174
  275.3 2.0 multiply_reduce_fusion
  277.4 2.8 fusion.87
  280.2 3.1 add_convert_fusion
  283.3 2.2 copy.90
  285.5 5.1 all-to-all-start
  290.7 48.5 %all-to-all-done = bf16[4,1024,512]{2,1,0:T(8,128)(2,1)} async-done(((bf16[4,1024,512]{2,1,0:T(8,128)(2,1)}), bf16[4,1024,512]{2,1,0:T(8,128)(2,1)}, u32[]{:S(2)}, u32[]{:S(2)}) %all-to-all-start) | async-done | bytes 4194336 | tf_op jit(solution)/shard_map/all_to_all | solution.py:54
  339.1 3.0 convert_reduce_fusion.1
  342.2 1.6 fusion.80
  344.4 3.3 all-to-all-start.1
  348.5 4.5 all-to-all-done.1
  354.4 111.0 %all-gather.11.cloned.1.call-done = bf16[1024,2048]{1,0:T(8,128)(2,1)} async-done(((bf16[1024,512]{1,0:T(8,128)(2,1)}), bf16[1024,2048]{1,0:T(8,128)(2,1)}) %all-gather.11.cloned.1.call-update) | async-done | bytes 4194320 | tf_op jit(solution)/shard_map/all_gather | solution.py:193
  465.4 8.1 %multiply_convert_fusion = bf16[1024,1024]{1,0:T(8,128)(2,1)S(1)} fusion(bf16[1024,2048]{1,0:T(8,128)(2,1)} %all-gather.11.cloned.1.call-done, bf16[2048,2048]{1,0:T(8,128)(2,1)} %all-gather.13.cloned.1.call-done), kind=kOutput, calls=%fused_computation.98 | convolution fusion | flops 4298113024 | bytes 10485760 | tf_op jit(solution)/shard_map/dot_general | solution.py:194
  473.5 4.8 fusion.63
  478.7 51.8 %all_to_all.15 = bf16[4,1024,512]{2,1,0:T(8,128)(2,1)S(1)} all-to-all(bf16[4,1024,512]{2,1,0:T(8,128)(2,1)S(1)} %bitcast.288), channel_id=1, replica_groups=mesh['sp'=32,'tp'=4] {'tp'}, dimensions={0} | all-to-all | bytes 8388608 | tf_op jit(solution)/shard_map/all_to_all | solution.py:54
  531.1 1.4 fusion.83
  (424 shorter events, 185.1 us)
Async XLA Ops:
  6.5 270.8 %copy-start = (bf16[512,2048]{1,0:T(8,128)(2,1)S(1)}, bf16[512,2048]{1,0:T(8,128)(2,1)}, u32[]{:S(2)}) copy-start(bf16[512,2048]{1,0:T(8,128)(2,1)} %param.35) | copy-start | bytes 6291460
  6.5 5.1 copy-start.10
  6.5 5.1 copy-start.11
  6.5 263.0 %all-gather.17.cloned.1.call-start = ((), (), s32[]{:S(2)}) async-start(), calls=%async_computation.6 | async-start | bytes 4325376 | tf_op jit(solution)/shard_map/all_gather | solution.py:27
  83.9 6.7 %copy-start.7 = (bf16[1024,256]{1,0:T(8,128)(2,1)S(1)}, bf16[1024,256]{1,0:T(8,128)(2,1)}, u32[]{:S(2)}) copy-start(bf16[1024,256]{1,0:T(8,128)(2,1)} %param.24) | copy-start | bytes 1572868
  84.6 184.9 %all-gather.15.cloned.1.call-start = ((), (), s32[]{:S(2)}) async-start(), calls=%async_computation.5 | async-start | bytes 8650752 | tf_op jit(solution)/shard_map/all_gather | solution.py:27
  91.6 8.2 %copy-start.8 = (bf16[1024,256]{1,0:T(8,128)(2,1)S(1)}, bf16[1024,256]{1,0:T(8,128)(2,1)}, u32[]{:S(2)}) copy-start(bf16[1024,256]{1,0:T(8,128)(2,1)} %param.25) | copy-start | bytes 1572868
  103.5 109.6 %copy-start.12 = (bf16[1024,64]{0,1:T(8,128)(2,1)S(1)}, bf16[1024,64]{0,1:T(8,128)(2,1)}, u32[]{:S(2)}) copy-start(bf16[1024,64]{0,1:T(8,128)(2,1)} %param.39) | copy-start | bytes 393220
  103.5 109.6 %copy-start.13 = (bf16[64,1024]{1,0:T(8,128)(2,1)S(1)}, bf16[64,1024]{1,0:T(8,128)(2,1)}, u32[]{:S(2)}) copy-start(bf16[64,1024]{1,0:T(8,128)(2,1)} %param.38) | copy-start | bytes 393220
  213.1 141.3 %all-gather.13.cloned.1.call-start = ((), (), s32[]{:S(2)}) async-start(), calls=%async_computation.4 | async-start | bytes 8650752 | tf_op jit(solution)/shard_map/all_gather | solution.py:16
  213.9 3.0 copy-start.3
  218.2 3.0 copy-start.4
  269.6 5.7 %copy-start.2 = (f32[1024,1,512]{0,2,1:T(8,128)S(1)}, f32[1024,1,512]{0,2,1:T(8,128)}, u32[]{:S(2)}) copy-start(f32[1024,1,512]{0,2,1:T(8,128)} %copy.34) | copy-start | bytes 6291460
  269.6 5.7 %copy-start.9 = (f32[16,64,1,128]{3,1,2,0:T(8,128)S(1)}, f32[16,64,1,128]{3,1,2,0:T(8,128)}, u32[]{:S(2)}) copy-start(f32[16,64,1,128]{3,1,2,0:T(8,128)} %get-tuple-element.194) | copy-start | bytes 1572868
  275.3 2.1 copy-start.6
  275.3 2.1 copy-start.16
  277.4 2.8 copy-start.5
  277.4 2.8 copy-start.15
  285.5 53.6 %all-to-all-start = ((bf16[4,1024,512]{2,1,0:T(8,128)(2,1)}), bf16[4,1024,512]{2,1,0:T(8,128)(2,1)}, u32[]{:S(2)}, u32[]{:S(2)}) async-start(bf16[4,1024,512]{2,1,0:T(8,128)(2,1)} %bitcast.287), calls=%async_computation | async-start | bytes 8388608 | tf_op jit(solution)/shard_map/all_to_all | solution.py:54
  344.4 8.6 %all-to-all-start.1 = ((f32[4,1024,1]{1,2,0:T(1,128)}), f32[4,1024,1]{1,2,0:T(1,128)S(1)}, u32[]{:S(2)}, u32[]{:S(2)}) async-start(f32[4,1024,1]{1,2,0:T(1,128)} %broadcast_in_dim.50), calls=%async_computation.1 | async-start | bytes 32768 | tf_op jit(solution)/shard_map/all_to_all | solution.py:60
  347.7 117.7 %all-gather.11.cloned.1.call-start = ((), (), s32[]{:S(2)}) async-start(), calls=%async_computation.3 | async-start | bytes 5242880 | tf_op jit(solution)/shard_map/all_gather | solution.py:193
  465.4 8.1 %copy-start.14 = (bf16[2048,2048]{1,0:T(8,128)(2,1)S(1)}, bf16[2048,2048]{1,0:T(8,128)(2,1)}, u32[]{:S(2)}) copy-start(bf16[2048,2048]{1,0:T(8,128)(2,1)} %all-gather.13.cloned.1.call-done) | copy-start | bytes 25165828
  530.4 2.1 copy-start.1
Sparse Core Ops, SparseCore 0:
  84.7 48.7 all-gather.16
  213.2 55.4 all-gather.14
  271.0 52.3 all-gather.12
  354.5 110.8 all-gather.10
where the time goes:
time: 545 us; the launch traced here: 539 us
  waiting for transfers between devices  164 us (30%)
  blocking collectives  98.6 us (18%)
  matrix products  91.9 us (17%)
  local copies, waits for them, and re-layouts  86.4 us (16%)
  other arithmetic  74.3 us (14%)
  between operations  13.5 us (2%)
  starting transfers between devices  8.53 us (2%)
    all_gather x1, waiting for transfers between devices, body(): normed = lax.all_gather(normed_cols, 'tp', axis=1, tiled=True)  111 us
    all_to_all x1, blocking collectives, sum_at_owner(): pieces = lax.all_to_all(split_up(array, dim, count), axis, 0, 0, tiled=True)  51.8 us
    all_to_all x1, waiting for transfers between devices, sum_at_owner(): pieces = lax.all_to_all(split_up(array, dim, count), axis, 0, 0, tiled=True)  48.5 us
    all_gather x2, blocking collectives, entering(): lax.all_gather(a.astype(kind), axis)  46.9 us
    dynamic_slice x48, local copies, waits for them, and re-layouts, block_pass(): lax.scan(advance, initial, (to_blocks(queries), to_blocks(keys_in), to_bl...  41.7 us
    dot_general x32, matrix products, advance(): outside = jnp.einsum('ihd,hde->ihe', scaled_q, memory, precision=HIGHEST)  22.1 us
    dot_general x32, matrix products, advance(): inside = jnp.einsum('hij,jhe->ihe', scores, block_v, precision=HIGHEST)  19.3 us
    dot_general x32, matrix products, advance(): jnp.einsum('jhd,jhe->hde', decayed_keys, block_v, precision=HIGHEST)  17.8 us
  transfers between devices with their start and end apart: 6, of which 3 were waited for; matrix products, arithmetic and copies ran while one was open for 30% of the time, Pallas kernels for 0%

commit v1 on v0

--- a/solution.py
+++ b/solution.py
@@ -190,7 +190,7 @@
     normed_cols = (stream_f * lax.rsqrt(squares / full_width + EPS) * gain_cols).astype(
         jnp.bfloat16
     )
-    normed = lax.all_gather(normed_cols, "tp", axis=1, tiled=True)
+    normed = jnp.concatenate(lax.all_gather(normed_cols, "tp"), axis=1)
     before_activation = jnp.dot(normed, up_whole, preferred_element_type=jnp.float32)
     hidden = jnp.square(jax.nn.relu(before_activation)).astype(jnp.bfloat16)
     down_terms = jnp.dot(hidden, down_whole, preferred_element_type=jnp.float32)

time: 545 us -> 605 us (1.11)
  waiting for transfers between devices: 164 us -> 213 us
  local copies, waits for them, and re-layouts: 86.4 us -> 94.9 us
    all_gather x1, waiting for transfers between devices: 0.02 us -> 49.1 us  [turned_gather(): lax.all_gather(both, axis, axis=0, tiled=True)]
    dot_general x1, matrix products: 4.8 us -> 14.4 us  [body(): down_terms = jnp.dot(hidden, down_whole, preferred_element_type=jnp.float32)]
    dot_general x1 -> x0, matrix products: 8.08 us -> none  [body(): jnp.dot(normed, up_whole, preferred_element_type=jnp.float32)]
    reshape x0 -> x1, local copies, waits for them, and re-layouts: none -> 6.28 us  [body(): normed = jnp.concatenate(lax.all_gather(normed_cols, 'tp'), axis=1)]
  transfers between devices with their start and end apart: 6 -> 6, of which waited for: 3 -> 5; matrix products, arithmetic and copies ran while one was open for 30% -> 24% of each run, Pallas kernels for 0% -> 0%
where the time goes in v1:
time: 605 us; the launch traced here: 599 us
  waiting for transfers between devices  213 us (35%)
  blocking collectives  100 us (17%)
  local copies, waits for them, and re-layouts  94.9 us (16%)
  matrix products  93.5 us (15%)
  other arithmetic  74.4 us (12%)
  between operations  13.5 us (2%)
  starting transfers between devices  8.45 us (1%)
    all_gather x1, waiting for transfers between devices, body(): normed = jnp.concatenate(lax.all_gather(normed_cols, 'tp'), axis=1)  110 us
    all_to_all x1, blocking collectives, sum_at_owner(): pieces = lax.all_to_all(split_up(array, dim, count), axis, 0, 0, tiled=True)  53.3 us
    all_gather x1, waiting for transfers between devices, turned_gather(): lax.all_gather(both, axis, axis=0, tiled=True)  49.1 us
    all_to_all x1, waiting for transfers between devices, sum_at_owner(): pieces = lax.all_to_all(split_up(array, dim, count), axis, 0, 0, tiled=True)  48.6 us
    all_gather x2, blocking collectives, entering(): lax.all_gather(a.astype(kind), axis)  46.8 us
    dynamic_slice x48, local copies, waits for them, and re-layouts, block_pass(): lax.scan(advance, initial, (to_blocks(queries), to_blocks(keys_in), to_bl...  41.7 us
    dot_general x32, matrix products, advance(): outside = jnp.einsum('ihd,hde->ihe', scaled_q, memory, precision=HIGHEST)  22.2 us
    dot_general x32, matrix products, advance(): inside = jnp.einsum('hij,jhe->ihe', scores, block_v, precision=HIGHEST)  19.4 us
  transfers between devices with their start and end apart: 6, of which 5 were waited for; matrix products, arithmetic and copies ran while one was open for 24% of the time, Pallas kernels for 0%

profile of v1, /device:TPU:0, one launch (start us, length us, event | category | flops | bytes accessed | tf_op | source)
XLA Modules:
  0.0 599.2 jit_solution(9157917397439504235)
XLA Ops:
  6.6 5.0 reshape.526
  13.8 1.6 broadcast.136.clone.1
  15.4 68.6 %while.51 = (s32[]{:T(128)}, f32[1,128,512]{2,1,0:T(8,128)S(1)}, f32[1,128]{1,0:T(1,128)S(1)}, f32[16,64,1,512]{3,1,2,0:T(8,128)}, f32[16,64,1,128]{3,1,2,0:T(8,...) while((s32[]{:T(128)}, f32[1,128,512]{2,1,0:T(8,128)S(1)}, ...), condition=%wide.region_5.6_spmd.clone, body=%wide.region_3.5_spmd.clone.sunk | while | flops 133005568 | bytes 2333321 | solution.py:98
  84.8 2.7 fusion.92
  87.5 3.3 reshape.507
  91.8 3.3 reshape.508
  95.1 4.9 reshape.524
  100.0 2.0 reshape.523
  102.0 1.6 broadcast.136.clone
  103.6 108.9 %while.50 = (s32[]{:T(128)}, f32[1,256,512]{2,1,0:T(8,128)S(1)}, f32[1,256]{1,0:T(1,128)S(1)}, f32[16,64,1,512]{3,1,2,0:T(8,128)}, f32[16,64,1,256]{3,1,2,0:T(8,...) while((s32[]{:T(128)}, f32[1,256,512]{2,1,0:T(8,128)S(1)}, ...), condition=%wide.region_2.3_spmd.clone, body=%wide.region_0.2_spmd.clone.sunk | while | flops 240787968 | bytes 3648133 | solution.py:98
  213.3 3.0 copy.39
  217.6 3.0 copy.41
  221.9 23.1 %all-gather.6 = bf16[32,1,128]{2,1,0:T(2,128)(2,1)S(1)} all-gather(bf16[1,1,128]{2,1,0:T(2,128)(2,1)S(1)} %convert_bitcast_fusion.1), channel_id=4, replica_groups=mesh['sp'=32,'tp'=4] {'sp'}, dimensions={0}, use_global_device_ids=true | all-gather | bytes 8448 | tf_op jit(solution)/shard_map/all_gather | solution.py:27
  245.0 23.7 %all-gather.5 = bf16[32,1,256]{2,1,0:T(2,128)(2,1)S(1)} all-gather(bf16[1,1,256]{2,1,0:T(2,128)(2,1)S(1)} %convert_bitcast_fusion), channel_id=2, replica_groups=mesh['sp'=32,'tp'=4] {'sp'}, dimensions={0}, use_global_device_ids=true | all-gather | bytes 16896 | tf_op jit(solution)/shard_map/all_gather | solution.py:27
  269.0 5.6 multiply_reduce_fusion.1
  274.7 2.0 multiply_reduce_fusion
  276.8 2.8 fusion.89
  279.6 3.1 add_convert_fusion
  282.6 2.3 copy.98
  285.0 5.1 all-to-all-start
  290.0 48.6 %all-to-all-done = bf16[4,1024,512]{2,1,0:T(8,128)(2,1)} async-done(((bf16[4,1024,512]{2,1,0:T(8,128)(2,1)}), bf16[4,1024,512]{2,1,0:T(8,128)(2,1)}, u32[]{:S(2)}, u32[]{:S(2)}) %all-to-all-start) | async-done | bytes 4194336 | tf_op jit(solution)/shard_map/all_to_all | solution.py:54
  338.6 3.0 convert_reduce_fusion.1
  341.7 1.6 fusion.80
  343.9 3.3 all-to-all-start.1
  348.0 4.6 all-to-all-done.1
  354.7 110.2 %all-gather.18.cloned.1.call-done = bf16[4096,512]{1,0:T(8,128)(2,1)} async-done(((bf16[1024,512]{1,0:T(8,128)(2,1)}), bf16[4096,512]{1,0:T(8,128)(2,1)}) %all-gather.18.cloned.1.call-update) | async-done | bytes 4194320 | tf_op jit(solution)/shard_map/all_gather | solution.py:193
  464.9 6.3 %copy.44 = bf16[1024,4,512]{0,2,1:T(8,128)(2,1)} copy(bf16[1024,4,512]{2,0,1:T(8,128)(2,1)} %bitcast.299) | data formatting | bytes 8388608 | tf_op jit(solution)/shard_map/reshape | solution.py:193
  471.2 49.1 %all-gather.12.cloned.1.call-done = bf16[2048,2048]{1,0:T(8,128)(2,1)} async-done(((bf16[64,2048]{1,0:T(8,128)(2,1)}), bf16[2048,2048]{1,0:T(8,128)(2,1)}) %all-gather.12.cloned.1.call-update) | async-done | bytes 8388624 | tf_op jit(solution)/shard_map/all_gather | solution.py:16
  520.3 14.4 %fusion.63 = bf16[1024,2048]{1,0:T(8,128)(2,1)} fusion(bf16[2048,2048]{1,0:T(8,128)(2,1)} %all-gather.12.cloned.1.call-done, bf16[1024,2048]{0,1:T(8,128)(2,1)} %bitcast.300), kind=kOutput, calls=%fused_computation.99 | convolution fusion | flops 8595177472 | bytes 16777216 | tf_op jit(solution)/shard_map/dot_general | solution.py:196
  534.7 2.6 copy.97
  537.3 53.3 %all_to_all.15 = bf16[4,1024,512]{2,1,0:T(8,128)(2,1)S(1)} all-to-all(bf16[4,1024,512]{2,1,0:T(8,128)(2,1)S(1)} %bitcast.291), channel_id=1, replica_groups=mesh['sp'=32,'tp'=4] {'tp'}, dimensions={0} | all-to-all | bytes 8388608 | tf_op jit(solution)/shard_map/all_to_all | solution.py:54
  591.2 1.4 fusion.83
  (422 shorter events, 187.8 us)
Async XLA Ops:
  6.5 270.2 %copy-start = (bf16[512,2048]{1,0:T(8,128)(2,1)S(1)}, bf16[512,2048]{1,0:T(8,128)(2,1)}, u32[]{:S(2)}) copy-start(bf16[512,2048]{1,0:T(8,128)(2,1)} %param.35) | copy-start | bytes 6291460
  6.5 5.1 copy-start.10
  6.5 5.1 copy-start.11
  6.5 262.1 %all-gather.16.cloned.1.call-start = ((), (), s32[]{:S(2)}) async-start(), calls=%async_computation.5 | async-start | bytes 4325376 | tf_op jit(solution)/shard_map/all_gather | solution.py:27
  84.0 6.8 %copy-start.7 = (bf16[1024,256]{1,0:T(8,128)(2,1)S(1)}, bf16[1024,256]{1,0:T(8,128)(2,1)}, u32[]{:S(2)}) copy-start(bf16[1024,256]{1,0:T(8,128)(2,1)} %param.24) | copy-start | bytes 1572868
  84.7 184.2 %all-gather.14.cloned.1.call-start = ((), (), s32[]{:S(2)}) async-start(), calls=%async_computation.4 | async-start | bytes 8650752 | tf_op jit(solution)/shard_map/all_gather | solution.py:27
  91.8 8.2 %copy-start.8 = (bf16[1024,256]{1,0:T(8,128)(2,1)S(1)}, bf16[1024,256]{1,0:T(8,128)(2,1)}, u32[]{:S(2)}) copy-start(bf16[1024,256]{1,0:T(8,128)(2,1)} %param.25) | copy-start | bytes 1572868
  213.3 3.0 copy-start.3
  217.6 3.0 copy-start.4
  269.0 5.7 copy-start.2
  269.0 5.7 copy-start.9
  274.7 2.1 copy-start.6
  274.7 2.1 copy-start.15
  276.8 2.8 copy-start.5
  276.8 2.8 copy-start.14
  285.0 53.7 %all-to-all-start = ((bf16[4,1024,512]{2,1,0:T(8,128)(2,1)}), bf16[4,1024,512]{2,1,0:T(8,128)(2,1)}, u32[]{:S(2)}, u32[]{:S(2)}) async-start(bf16[4,1024,512]{2,1,0:T(8,128)(2,1)} %bitcast.290), calls=%async_computation | async-start | bytes 8388608 | tf_op jit(solution)/shard_map/all_to_all | solution.py:54
  343.3 10.7 %copy-start.12 = (bf16[1024,64]{0,1:T(8,128)(2,1)S(1)}, bf16[1024,64]{0,1:T(8,128)(2,1)}, u32[]{:S(2)}) copy-start(bf16[1024,64]{0,1:T(8,128)(2,1)} %param.39) | copy-start | bytes 393220
  343.3 10.7 %copy-start.13 = (bf16[64,1024]{1,0:T(8,128)(2,1)S(1)}, bf16[64,1024]{1,0:T(8,128)(2,1)}, u32[]{:S(2)}) copy-start(bf16[64,1024]{1,0:T(8,128)(2,1)} %param.38) | copy-start | bytes 393220
  343.9 8.6 %all-to-all-start.1 = ((f32[4,1024,1]{1,2,0:T(1,128)}), f32[4,1024,1]{1,2,0:T(1,128)S(1)}, u32[]{:S(2)}, u32[]{:S(2)}) async-start(f32[4,1024,1]{1,2,0:T(1,128)} %broadcast_in_dim.50), calls=%async_computation.1 | async-start | bytes 32768 | tf_op jit(solution)/shard_map/all_to_all | solution.py:60
  347.2 117.8 %all-gather.18.cloned.1.call-start = ((), (), s32[]{:S(2)}) async-start(), calls=%async_computation.6 | async-start | bytes 5242880 | tf_op jit(solution)/shard_map/all_gather | solution.py:193
  353.9 166.4 %all-gather.12.cloned.1.call-start = ((), (), s32[]{:S(2)}) async-start(), calls=%async_computation.3 | async-start | bytes 8650752 | tf_op jit(solution)/shard_map/all_gather | solution.py:16
  590.6 2.1 copy-start.1
Sparse Core Ops, SparseCore 0:
  84.8 48.6 all-gather.15
  213.4 55.4 all-gather.13
  354.0 110.8 all-gather.17
  467.1 53.2 all-gather.11
